TPU v7x, 32 devices: a whole 2x2x4 slice. The times are simulated.
32 devices in a mesh: sp: 8 (over z, x), tp: 4 (over y, core).
Axes of the slice: x: 2, y: 2, z: 4, core: 2. Of those that a mesh axis runs over, the one named last changes fastest.
Arguments:
- query_small: bfloat16 [6144, 1024], P('sp', 'tp'), may hold values from -6 to 6
- key_small: bfloat16 [6144, 1024], P('sp', 'tp'), may hold values from -6 to 6
- value_small: bfloat16 [6144, 1024], P('sp', 'tp'), may hold values from -6 to 6
- gates_small: float32 [6144, 16], P('sp', 'tp'), as said below
- query_large: bfloat16 [6144, 1024], P('sp', 'tp'), may hold values from -6 to 6
- key_large: bfloat16 [6144, 1024], P('sp', 'tp'), may hold values from -6 to 6
- value_large: bfloat16 [6144, 1024], P('sp', 'tp'), may hold values from -6 to 6
- gates_large: float32 [6144, 8], P('sp', 'tp'), as said below
- residual: bfloat16 [6144, 2048], P(('sp', 'tp')), may hold values from -6 to 6
- mixer_small: bfloat16 [1024, 2048], P('tp'), may hold values from -1 to 1
- mixer_large: bfloat16 [1024, 2048], P('tp'), may hold values from -1 to 1
- mix_gain: float32 [2048], replicated, may hold values from 0.1 to 1.9
- value_weight: bfloat16 [2048, 5632], P('sp', 'tp'), may hold values from -0.125 to 0.125
- gate_weight: bfloat16 [2048, 5632], P('sp', 'tp'), may hold values from -0.125 to 0.125
- value_taps: float32 [3, 5632], P(None, 'tp'), may hold values from -3 to 3
- gate_taps: float32 [3, 5632], P(None, 'tp'), may hold values from -3 to 3
- down_weight: bfloat16 [5632, 2048], P('tp', 'sp'), may hold values from -0.078125 to 0.078125
- final_gain: float32 [2048], replicated, may hold values from 0.1 to 1.9
Outputs:
- layer_out: bfloat16 [6144, 2048], P(('sp', 'tp'))
Inputs may be any that keep to these rules, and one draw needn't show every extreme that they name: `gates_small`: each column never rises from one position to the next, and its first entry is negative. `gates_large`: each column never rises from one position to the next, and its first entry is negative.
All inputs are finite; a program needn't handle non-finite values.
Results may differ from a plain program's by a relative error of at most 0.018.
Values may be sent and summed in bfloat16 or wider, within the bound.
A program may use at most 128 MiB of HBM per device.

v0:
```python
import math

import jax
import jax.numpy as jnp
from jax import lax
from jax.sharding import PartitionSpec as P

DS = 64
DL = 128


residual_scale = 2.0**0.5
epsilon = 1e-05


def passed_along(value, axis, steps):
    count = lax.axis_size(axis)
    first, last = (max(0, -steps), min(count, count - steps))
    return lax.ppermute(value, axis, [(source, source + steps) for source in range(first, last)])


def norm_rows(values, gain):
    center = jnp.mean(values, axis=-1, keepdims=True)
    spread = jnp.mean(jnp.square(values - center), axis=-1, keepdims=True)
    return (values - center) * lax.rsqrt(spread + epsilon) * gain


def attend_block(
    running,
    queries,
    query_gates,
    key_rows,
    value_rows,
    key_gates,
    token_positions,
    key_first,
    head_dim,
):
    running_peak, weight_sum, weighted = running
    heads_here = query_gates.shape[1]
    span_rows = key_rows.shape[0]
    query_heads = queries.reshape(queries.shape[0], heads_here, head_dim)
    key_heads = key_rows.reshape(span_rows, heads_here, head_dim)
    value_heads = value_rows.reshape(span_rows, heads_here, head_dim)
    scores = jnp.einsum(
        "qhd,khd->hqk", query_heads, key_heads, preferred_element_type=jnp.float32
    ) * head_dim ** (-0.5)
    scores = scores + query_gates.T[:, :, None] - key_gates.T[:, None, :]
    key_positions = key_first + jnp.arange(span_rows)
    allowed = token_positions[:, None] >= key_positions[None, :]
    scores = jnp.where(allowed[None], scores, -1e30)
    new_peak = jnp.maximum(running_peak, jnp.max(scores, axis=-1))
    factor = jnp.exp(running_peak - new_peak)
    weights = jnp.where(allowed[None], jnp.exp(scores - new_peak[:, :, None]), 0.0)
    weight_sum = weight_sum * factor + jnp.sum(weights, axis=-1)
    update = jnp.einsum(
        "hqk,khd->qhd",
        weights.astype(jnp.bfloat16),
        value_heads,
        preferred_element_type=jnp.float32,
    )
    weighted = weighted * factor.T[:, :, None] + update
    return (new_peak, weight_sum, weighted)


def per_device(
    query_small,
    key_small,
    value_small,
    gates_small,
    query_large,
    key_large,
    value_large,
    gates_large,
    residual,
    mixer_small,
    mixer_large,
    mix_gain,
    value_weight,
    gate_weight,
    value_taps,
    gate_taps,
    down_weight,
    final_gain,
):
    shard_rows = query_small.shape[0]
    first_row = lax.axis_index("sp") * shard_rows
    token_positions = first_row + jnp.arange(shard_rows)
    last_position = first_row + shard_rows - 1
    every_gate = (
        lax.all_gather(gates_small, "sp", axis=0, tiled=True),
        lax.all_gather(gates_large, "sp", axis=0, tiled=True),
    )
    heads_small = gates_small.shape[1]
    heads_large = gates_large.shape[1]

    def fresh(heads_here, head_dim):
        return (
            jnp.full((heads_here, shard_rows), -1e30, jnp.float32),
            jnp.zeros((heads_here, shard_rows), jnp.float32),
            jnp.zeros((shard_rows, heads_here, head_dim), jnp.float32),
        )

    pieces = (
        lax.all_gather(key_small, "sp", axis=0, tiled=True),
        lax.all_gather(value_small, "sp", axis=0, tiled=True),
        lax.all_gather(key_large, "sp", axis=0, tiled=True),
        lax.all_gather(value_large, "sp", axis=0, tiled=True),
    )
    span_total = pieces[0].shape[0]
    block_rows = shard_rows * math.gcd(span_total // shard_rows, max(1, 1024 // shard_rows))

    def one_block(block_index, current):
        offset = block_index * block_rows
        sliced = [lax.dynamic_slice_in_dim(member, offset, block_rows, 0) for member in pieces]
        gate_small = lax.dynamic_slice_in_dim(every_gate[0], offset, block_rows, 0)
        gate_large = lax.dynamic_slice_in_dim(every_gate[1], offset, block_rows, 0)

        def update(previous):
            return (
                attend_block(
                    previous[0],
                    query_small,
                    gates_small,
                    sliced[0],
                    sliced[1],
                    gate_small,
                    token_positions,
                    offset,
                    DS,
                ),
                attend_block(
                    previous[1],
                    query_large,
                    gates_large,
                    sliced[2],
                    sliced[3],
                    gate_large,
                    token_positions,
                    offset,
                    DL,
                ),
            )

        def unchanged(previous):
            return previous

        return lax.cond(offset <= last_position, update, unchanged, current)

    block_count = span_total // block_rows
    small_state, large_state = lax.fori_loop(
        0, block_count, one_block, (fresh(heads_small, DS), fresh(heads_large, DL))
    )
    small_out = (
        (small_state[2] / small_state[1].T[:, :, None])
        .reshape(shard_rows, heads_small * DS)
        .astype(jnp.bfloat16)
    )
    large_out = (
        (large_state[2] / large_state[1].T[:, :, None])
        .reshape(shard_rows, heads_large * DL)
        .astype(jnp.bfloat16)
    )
    tensor_parts = lax.axis_size("tp")
    own_rows = shard_rows // tensor_parts
    joined = jnp.concatenate([small_out, large_out], axis=1)
    arrived = lax.all_to_all(joined, "tp", split_axis=0, concat_axis=1, tiled=True)
    layout = arrived.reshape(own_rows, tensor_parts, joined.shape[1])
    small_width = small_out.shape[1]
    all_small = layout[:, :, :small_width].reshape(own_rows, tensor_parts * small_width)
    all_large = layout[:, :, small_width:].reshape(own_rows, tensor_parts * large_out.shape[1])
    mix = jnp.dot(
        all_small,
        lax.all_gather(mixer_small, "tp", axis=0, tiled=True),
        preferred_element_type=jnp.float32,
    ) + jnp.dot(
        all_large,
        lax.all_gather(mixer_large, "tp", axis=0, tiled=True),
        preferred_element_type=jnp.float32,
    )
    mixed = norm_rows(residual_scale * residual.astype(jnp.float32) + mix, mix_gain).astype(
        jnp.bfloat16
    )
    block_input = lax.all_gather(mixed, "tp", axis=0, tiled=True)

    def add_up(pieces):
        return (
            jnp.dot(block_input, pieces[0], preferred_element_type=jnp.float32),
            jnp.dot(block_input, pieces[1], preferred_element_type=jnp.float32),
        )

    up_value, up_gate = add_up(
        (
            lax.all_gather(value_weight, "sp", axis=0, tiled=True),
            lax.all_gather(gate_weight, "sp", axis=0, tiled=True),
        )
    )
    up_value = up_value.astype(jnp.bfloat16)
    up_gate = up_gate.astype(jnp.bfloat16)
    hidden_width = up_value.shape[1]
    trailing = jnp.concatenate([up_value[-2:], up_gate[-2:]], axis=1)
    earlier = passed_along(trailing, "sp", 1)
    padded_value = jnp.concatenate([earlier[:, :hidden_width], up_value], axis=0).astype(
        jnp.float32
    )
    padded_gate = jnp.concatenate([earlier[:, hidden_width:], up_gate], axis=0).astype(jnp.float32)
    filt_value = (
        value_taps[0] * padded_value[:-2]
        + value_taps[1] * padded_value[1:-1]
        + value_taps[2] * padded_value[2:]
    )
    filt_gate = (
        gate_taps[0] * padded_gate[:-2]
        + gate_taps[1] * padded_gate[1:-1]
        + gate_taps[2] * padded_gate[2:]
    )
    hidden = (jax.nn.silu(filt_gate) * filt_value).astype(jnp.bfloat16)
    ffn_terms = jnp.dot(
        hidden,
        lax.all_gather(down_weight, "sp", axis=1, tiled=True),
        preferred_element_type=jnp.float32,
    )
    ffn = lax.psum_scatter(
        ffn_terms.astype(jnp.bfloat16), "tp", scatter_dimension=0, tiled=True
    ).astype(jnp.float32)
    return norm_rows(residual_scale * mixed.astype(jnp.float32) + ffn, final_gain).astype(
        jnp.bfloat16
    )


def solution(mesh):
    in_specs = (
        P("sp", "tp"),
        P("sp", "tp"),
        P("sp", "tp"),
        P("sp", "tp"),
        P("sp", "tp"),
        P("sp", "tp"),
        P("sp", "tp"),
        P("sp", "tp"),
        P(("sp", "tp"), None),
        P("tp", None),
        P("tp", None),
        P(),
        P("sp", "tp"),
        P("sp", "tp"),
        P(None, "tp"),
        P(None, "tp"),
        P("tp", "sp"),
        P(),
    )
    out_specs = P(("sp", "tp"), None)
    return jax.shard_map(
        per_device, mesh=mesh, in_specs=in_specs, out_specs=out_specs, check_vma=False
    )
```

profile of v0, /device:TPU:0, one launch (start us, length us, event | category | flops | bytes accessed | tf_op | source)
XLA Modules:
  0.0 712.8 jit_solution(5404534390486293177)
XLA Ops:
  6.5 2.0 copy.44
  8.5 0.0 all-gather.13.cloned.1.call-start
  8.6 2.0 copy.45
  10.6 0.0 all-gather.15.cloned.1.call-start
  10.6 2.0 copy.46
  12.6 0.0 all-gather.17.cloned.1.call-start
  12.7 1.9 copy.47
  14.6 0.0 all-gather.19.cloned.1.call-start
  14.7 0.5 all-gather.19.cloned.1.call-update
  15.3 0.5 all-gather.21.cloned.1.call-update
  15.8 0.7 all-gather.25.cloned.1.call-update
  16.5 0.0 all-gather.23.cloned.1.call-start
  16.6 0.2 copy.48
  16.8 33.1 %all_gather.40 = f32[6144,2]{0,1:T(2,128)S(1)} all-gather(f32[768,2]{0,1:T(2,128)S(1)} %copy-done.5), channel_id=1, replica_groups=mesh['sp'=8,'tp'=4] {'sp'}, dimensions={0}, use_global_device_ids=true | all-gather | bytes 55296 | tf_op jit(solution)/shard_map/all_gather | solution.py:92
  49.9 31.3 %all_gather.37 = f32[6144,4]{0,1:T(4,128)S(1)} all-gather(f32[768,4]{0,1:T(4,128)S(1)} %copy-done.3), channel_id=1, replica_groups=mesh['sp'=8,'tp'=4] {'sp'}, dimensions={0}, use_global_device_ids=true | all-gather | bytes 110592 | tf_op jit(solution)/shard_map/all_gather | solution.py:91
  81.2 53.8 %all-gather.13.cloned.1.call-done = bf16[6144,256]{0,1:T(8,128)(2,1)} async-done(((bf16[768,256]{0,1:T(8,128)(2,1)}), bf16[6144,256]{0,1:T(8,128)(2,1)}) %all-gather.13.cloned.1.call-update) | async-done | bytes 3145744 | tf_op jit(solution)/shard_map/all_gather | solution.py:106
  135.0 61.0 %all-gather.15.cloned.1.call-done = bf16[6144,256]{0,1:T(8,128)(2,1)} async-done(((bf16[768,256]{0,1:T(8,128)(2,1)}), bf16[6144,256]{0,1:T(8,128)(2,1)}) %all-gather.15.cloned.1.call-update) | async-done | bytes 3145744 | tf_op jit(solution)/shard_map/all_gather | solution.py:107
  196.0 60.8 %all-gather.17.cloned.1.call-done = bf16[6144,256]{0,1:T(8,128)(2,1)} async-done(((bf16[768,256]{0,1:T(8,128)(2,1)}), bf16[6144,256]{0,1:T(8,128)(2,1)}) %all-gather.17.cloned.1.call-update) | async-done | bytes 3145744 | tf_op jit(solution)/shard_map/all_gather | solution.py:108
  256.8 0.1 broadcast_in_dim.102
  256.9 0.1 broadcast_in_dim.99
  257.0 19.2 %while.24 = (s32[]{:T(128)}, f32[4,768]{1,0:T(4,128)S(1)}, f32[4,768]{1,0:T(4,128)S(1)}, f32[768,4,64]{0,2,1:T(8,128)S(1)}, f32[2,768]{1,0:T(2,128)S(1)}, /*inde...) while((s32[]{:T(128)}, f32[4,768]{1,0:T(4,128)S(1)}, ...), condition=%wide.region_7.8_spmd.clone, body=%wide.region_0.7_spmd.clone.sunk | while | flops 1276591104 | bytes 55708176 | solution.py:151
  257.0 18.5 %conditional.3 = ((f32[4,768]{1,0:T(4,128)S(1)}, f32[4,768]{1,0:T(4,128)S(1)}, f32[768,4,64]{0,2,1:T(8,128)S(1)}, f32[2,768]{1,0:T(2,128)S(1)}, f32[2,768]{1,0:T(2,128)S(1)}, /*index=5*/f32[768,2,128]{2,0,1:T(8,128)S(1)})) conditional(s32[]{:T(128)} %convert_element_type.127, (f32[4,768]{1,0:T(4,128)S(1)}, f32[4,768]{1,0:T(4,128)S(1)}, ...), branch_computations={%region_1.0_spmd, %region_2.6_spmd} | conditional | flops 1276591104 | bytes 55704688 | solution.py:148
  257.1 1.2 constant_dynamic-slice_fusion
  258.3 0.4 broadcast_compare_fusion
  258.7 1.5 fusion.10
  260.2 2.5 fusion.20
  262.7 1.7 fusion.9
  264.5 1.2 constant_dynamic-slice_fusion.2
  265.7 2.7 fusion.4
  268.5 3.6 fusion.23
  272.1 3.5 fusion.3
  276.2 0.1 divide_convert_fusion.1
  276.2 0.5 convert_element_type.68
  276.7 0.3 divide_convert_fusion
  277.0 0.2 copy.58
  277.2 0.5 reshape.124
  277.7 0.7 pad_maximum_fusion
  278.4 0.7 copy.51
  279.1 19.0 %all_to_all.13 = bf16[4,192,512]{2,1,0:T(8,128)(2,1)S(1)} all-to-all(bf16[4,192,512]{2,1,0:T(8,128)(2,1)S(1)} %copy.51), channel_id=1, replica_groups=mesh['sp'=8,'tp'=4] {'tp'}, dimensions={0} | all-to-all | bytes 1572864 | tf_op jit(solution)/shard_map/all_to_all | solution.py:167
  298.1 0.1 slice_bitcast_fusion
  298.3 3.5 fusion.49
  301.8 26.2 %all-gather.21.cloned.1.call-done = bf16[1024,2048]{1,0:T(8,128)(2,1)} async-done(((bf16[256,2048]{1,0:T(8,128)(2,1)}), bf16[1024,2048]{1,0:T(8,128)(2,1)}) %all-gather.21.cloned.1.call-update) | async-done | bytes 4194320 | tf_op jit(solution)/shard_map/all_gather | solution.py:178
  328.0 3.6 fusion.48
  331.6 0.3 multiply_reduce_fusion.1
  331.9 1.2 multiply_convert_fusion.1
  333.1 0.0 all-gather.27.cloned.1.call-start
  333.2 0.7 all-gather.27.cloned.1.call-update
  333.9 0.5 all-gather.29.cloned.1.call-update
  334.5 92.2 %all-gather.25.cloned.1.call-done = bf16[2048,1408]{1,0:T(8,128)(2,1)} async-done(((bf16[256,1408]{1,0:T(8,128)(2,1)}), bf16[2048,1408]{1,0:T(8,128)(2,1)}) %all-gather.25.cloned.1.call-update) | async-done | bytes 5767184 | tf_op jit(solution)/shard_map/all_gather | solution.py:194
  426.7 30.9 %all-gather.23.cloned.1.call-done = bf16[768,2048]{1,0:T(8,128)(2,1)} async-done(((bf16[192,2048]{1,0:T(8,128)(2,1)}), bf16[768,2048]{1,0:T(8,128)(2,1)}) %all-gather.23.cloned.1.call-update) | async-done | bytes 3145744 | tf_op jit(solution)/shard_map/all_gather | solution.py:184
  457.6 8.3 %convolution_convert_fusion.2 = bf16[768,1408]{1,0:T(8,128)(2,1)S(1)} fusion(bf16[768,2048]{1,0:T(8,128)(2,1)} %all-gather.23.cloned.1.call-done, bf16[2048,1408]{1,0:T(8,128)(2,1)} %all-gather.25.cloned.1.call-done), kind=kOutput, calls=%fused_computation.57 | convolution fusion | flops 4430266368 | bytes 11075584 | tf_op jit(solution)/shard_map/dot_general | solution.py:188
  465.9 1.3 copy-done.1
  467.3 84.8 %all-gather.27.cloned.1.call-done = bf16[2048,1408]{1,0:T(8,128)(2,1)} async-done(((bf16[256,1408]{1,0:T(8,128)(2,1)}), bf16[2048,1408]{1,0:T(8,128)(2,1)}) %all-gather.27.cloned.1.call-update) | async-done | bytes 5767184 | tf_op jit(solution)/shard_map/all_gather | solution.py:195
  552.1 8.5 %convolution_convert_fusion.1 = bf16[768,1408]{1,0:T(8,128)(2,1)S(1)} fusion(bf16[768,2048]{1,0:T(8,128)(2,1)} %all-gather.23.cloned.1.call-done, bf16[2048,1408]{1,0:T(8,128)(2,1)} %all-gather.27.cloned.1.call-done), kind=kOutput, calls=%fused_computation.56 | convolution fusion | flops 4430266368 | bytes 11075584 | tf_op jit(solution)/shard_map/dot_general | solution.py:189
  560.6 2.5 collective-permute-start
  563.1 0.1 slice_reduce_fusion.2
  563.2 1.4 collective-permute-done
  564.6 4.2 maximum_convert_fusion
  568.9 76.7 %all-gather.29.cloned.1.call-done = bf16[1408,2048]{1,0:T(8,128)(2,1)} async-done(((bf16[1408,256]{1,0:T(8,128)(2,1)}), bf16[1408,2048]{1,0:T(8,128)(2,1)}) %all-gather.29.cloned.1.call-update) | async-done | bytes 5767184 | tf_op jit(solution)/shard_map/all_gather | solution.py:220
  645.6 19.1 %convolution_convert_fusion = bf16[768,2048]{1,0:T(8,128)(2,1)} fusion(bf16[1408,2048]{1,0:T(8,128)(2,1)} %all-gather.29.cloned.1.call-done, f32[770,1408]{1,0:T(8,128)} %get-tuple-element.726, f32[770,1408]{1,0:T(8,128)} %get-tuple-element.725, f32[1408]{0:T(1024)S(1)} %get-tuple-element.665, f32[1408]{0:T(1024)S(1)} %get-tuple-element.666, ...), kind=kOutput, calls=%fused_computation.55 | convolution fusion | flops 4448059392 | bytes 34898944 | tf_op jit(solution)/shard_map/dot_general | solution.py:218
  664.7 36.2 %reduce-scatter.2.cloned.1.call-done = bf16[192,2048]{1,0:T(8,128)(2,1)} async-done(((bf16[768,2048]{1,0:T(8,128)(2,1)}), bf16[192,2048]{1,0:T(8,128)(2,1)}) %reduce-scatter.2.cloned.1.call-update) | async-done | bytes 786448 | tf_op jit(solution)/shard_map/reduce_scatter | solution.py:223
  700.9 1.7 fusion.45
  702.7 1.7 multiply_reduce_fusion
  704.4 1.8 multiply_convert_fusion
  (72 shorter events, 0.7 us)
Async XLA Ops:
  6.5 10.1 %copy-start.4 = (bf16[768,256]{1,0:T(8,128)(2,1)S(1)}, bf16[768,256]{1,0:T(8,128)(2,1)}, u32[]{:S(2)}) copy-start(bf16[768,256]{1,0:T(8,128)(2,1)} %param.22) | copy-start | bytes 1179652
  6.5 10.2 %copy-start.5 = (f32[768,2]{0,1:T(2,128)S(1)}, f32[768,2]{0,1:T(2,128)}, u32[]{:S(2)}) copy-start(f32[768,2]{0,1:T(2,128)} %param.29) | copy-start | bytes 18436
  6.5 43.4 %copy-start.3 = (f32[768,4]{0,1:T(4,128)S(1)}, f32[768,4]{0,1:T(4,128)}, u32[]{:S(2)}) copy-start(f32[768,4]{0,1:T(4,128)} %param.25) | copy-start | bytes 36868
  6.5 74.7 %all-gather.11.cloned.1.call-start = ((), (), s32[]{:S(2)}) async-start(), calls=%async_computation.2 | async-start | bytes 3538944 | tf_op jit(solution)/shard_map/all_gather | solution.py:105
  8.5 248.5 %copy-start.10 = (bf16[768,256]{1,0:T(8,128)(2,1)S(1)}, bf16[768,256]{1,0:T(8,128)(2,1)}, u32[]{:S(2)}) copy-start(bf16[768,256]{1,0:T(8,128)(2,1)} %param.26) | copy-start | bytes 1179652
  8.5 126.5 %all-gather.13.cloned.1.call-start = ((), (), s32[]{:S(2)}) async-start(), calls=%async_computation.3 | async-start | bytes 3538944 | tf_op jit(solution)/shard_map/all_gather | solution.py:106
  10.6 185.4 %all-gather.15.cloned.1.call-start = ((), (), s32[]{:S(2)}) async-start(), calls=%async_computation.4 | async-start | bytes 3538944 | tf_op jit(solution)/shard_map/all_gather | solution.py:107
  12.6 244.2 %all-gather.17.cloned.1.call-start = ((), (), s32[]{:S(2)}) async-start(), calls=%async_computation.5 | async-start | bytes 3538944 | tf_op jit(solution)/shard_map/all_gather | solution.py:108
  14.6 283.6 %all-gather.19.cloned.1.call-start = ((), (), s32[]{:S(2)}) async-start(), calls=%async_computation.6 | async-start | bytes 5242880 | tf_op jit(solution)/shard_map/all_gather | solution.py:174
  15.2 312.8 %all-gather.21.cloned.1.call-start = ((), (), s32[]{:S(2)}) async-start(), calls=%async_computation.7 | async-start | bytes 5242880 | tf_op jit(solution)/shard_map/all_gather | solution.py:178
  15.8 410.9 %all-gather.25.cloned.1.call-start = ((), (), s32[]{:S(2)}) async-start(), calls=%async_computation.9 | async-start | bytes 6488064 | tf_op jit(solution)/shard_map/all_gather | solution.py:194
  16.5 441.0 %all-gather.23.cloned.1.call-start = ((), (), s32[]{:S(2)}) async-start(), calls=%async_computation.8 | async-start | bytes 3932160 | tf_op jit(solution)/shard_map/all_gather | solution.py:184
  328.0 3.9 copy-start.6
  333.1 218.9 %all-gather.27.cloned.1.call-start = ((), (), s32[]{:S(2)}) async-start(), calls=%async_computation.10 | async-start | bytes 6488064 | tf_op jit(solution)/shard_map/all_gather | solution.py:195
  333.9 311.7 %all-gather.29.cloned.1.call-start = ((), (), s32[]{:S(2)}) async-start(), calls=%async_computation.11 | async-start | bytes 6488064 | tf_op jit(solution)/shard_map/all_gather | solution.py:220
  334.5 366.5 %reduce-scatter.2.cloned.1.call-start = ((), (), s32[]{:S(2)}) async-start(), calls=%async_computation.12 | async-start | bytes 3932160 | tf_op jit(solution)/shard_map/reduce_scatter | solution.py:223
  465.9 1.4 copy-start.1
  467.3 95.8 %copy-start.7 = (f32[3,1408]{1,0:T(4,128)S(1)}, f32[3,1408]{1,0:T(4,128)}, u32[]{:S(2)}) copy-start(f32[3,1408]{1,0:T(4,128)} %param.36) | copy-start | bytes 50692
  467.3 95.8 %copy-start.8 = (f32[3,1408]{1,0:T(4,128)S(1)}, f32[3,1408]{1,0:T(4,128)}, u32[]{:S(2)}) copy-start(f32[3,1408]{1,0:T(4,128)} %param.37) | copy-start | bytes 50692
  552.1 12.6 %copy-start.2 = (bf16[768,1408]{1,0:T(8,128)(2,1)S(1)}, bf16[768,1408]{1,0:T(8,128)(2,1)}, u32[]{:S(2)}) copy-start(bf16[768,1408]{1,0:T(8,128)(2,1)} %copy-done.1) | copy-start | bytes 6488068
  560.6 4.0 collective-permute-start
  664.7 39.7 %copy-start.9 = (f32[2048]{0:T(1024)S(1)}, f32[2048]{0:T(1024)}, u32[]{:S(2)}) copy-start(f32[2048]{0:T(1024)} %param.39) | copy-start | bytes 24580
  700.9 3.5 copy-start
Sparse Core Ops, SparseCore 0:
  9.6 64.2 all-gather.10
  76.1 58.8 all-gather.12
  137.3 58.6 all-gather.14
  198.1 58.6 all-gather.16
  258.2 37.8 all-gather.18
  297.5 30.4 all-gather.20
  330.2 96.4 all-gather.24
  428.2 29.2 all-gather.22
  459.7 92.2 all-gather.26
  554.0 91.6 all-gather.28
  664.8 36.0 reduce-scatter.1
where the time goes:
time: 714 us; the launch traced here: 713 us
  waiting for transfers between devices  527 us (74%)
  blocking collectives  83.4 us (12%)
  matrix products  53.3 us (7%)
  other arithmetic  17.8 us (2%)
  local copies, waits for them, and re-layouts  14 us (2%)
  between operations  13.6 us (2%)
    all_gather x1, waiting for transfers between devices, per_device(): lax.all_gather(value_weight, 'sp', axis=0, tiled=True)  92.2 us
    all_gather x1, waiting for transfers between devices, per_device(): lax.all_gather(gate_weight, 'sp', axis=0, tiled=True)  84.8 us
    all_gather x1, waiting for transfers between devices, per_device(): lax.all_gather(down_weight, 'sp', axis=1, tiled=True)  76.7 us
    all_gather x1, waiting for transfers between devices, per_device(): lax.all_gather(key_large, 'sp', axis=0, tiled=True)  61 us
    all_gather x1, waiting for transfers between devices, per_device(): lax.all_gather(value_large, 'sp', axis=0, tiled=True)  60.8 us
    all_gather x1, waiting for transfers between devices, per_device(): lax.all_gather(value_small, 'sp', axis=0, tiled=True)  53.8 us
    reduce_scatter x1, waiting for transfers between devices, per_device(): lax.psum_scatter(ffn_terms.astype(jnp.bfloat16), 'tp', scatter_dimension=...  36.2 us
    all_gather x1, blocking collectives, per_device(): lax.all_gather(gates_large, 'sp', axis=0, tiled=True)  33.1 us
  transfers between devices with their start and end apart: 12, of which 10 were waited for; matrix products, arithmetic and copies ran while one was open for 8% of the time, Pallas kernels for 0%

commit v1 on v0

v1 whole, which is shorter than its diff:
```python
import jax
import jax.numpy as jnp
from jax import lax
from jax.experimental import pallas as pl
from jax.experimental.pallas import tpu as pltpu
from jax.sharding import PartitionSpec as P


DS = 64
DL = 128


residual_scale = 2.0**0.5
epsilon = 1e-05


def passed_along(value, axis, steps):
    count = lax.axis_size(axis)
    first, last = (max(0, -steps), min(count, count - steps))
    return lax.ppermute(value, axis, [(source, source + steps) for source in range(first, last)])


def rotated(value, axis, steps):
    count = lax.axis_size(axis)
    return lax.ppermute(value, axis, [(s, (s + steps) % count) for s in range(count)])


def swapped(value, axis):
    return lax.ppermute(value, axis, [(s, s ^ 1) for s in range(lax.axis_size(axis))])


def norm_rows(values, gain):
    center = jnp.mean(values, axis=-1, keepdims=True)
    spread = jnp.mean(jnp.square(values - center), axis=-1, keepdims=True)
    return (values - center) * lax.rsqrt(spread + epsilon) * gain


def attend_body(small_count, diagonal, *refs):
    if diagonal:
        q_ref, k_ref, v_ref, gk_ref, gq_ref, peak_out, sum_out, acc_out = refs
    else:
        valid_ref, q_ref, k_ref, v_ref, gk_ref, gq_ref = refs[:6]
        peak_in, sum_in, acc_in, peak_out, sum_out, acc_out = refs[6:]
    head = pl.program_id(0)
    scale = jnp.where(head < small_count, DS ** (-0.5), DL ** (-0.5)).astype(jnp.float32)

    def logits():
        scores = lax.dot_general(
            q_ref[0], k_ref[...], (((1,), (1,)), ((), ())), preferred_element_type=jnp.float32
        )
        return scores * scale + (gq_ref[0] - gk_ref[0])

    if diagonal:
        scores = logits()
        query_rows = pl.program_id(1) * scores.shape[0]
        allowed = query_rows + lax.broadcasted_iota(
            jnp.int32, scores.shape, 0
        ) >= lax.broadcasted_iota(jnp.int32, scores.shape, 1)
        scores = jnp.where(allowed, scores, -jnp.inf)
        peak = jnp.max(scores, axis=-1, keepdims=True)
        weights = jnp.exp(scores - peak)
        peak_out[0] = peak
        sum_out[0] = jnp.sum(weights, axis=-1, keepdims=True)
        acc_out[0] = jnp.dot(
            weights.astype(jnp.bfloat16), v_ref[...], preferred_element_type=jnp.float32
        )
        return

    @pl.when(valid_ref[0] > 0)
    def _():
        scores = logits()
        peak = jnp.maximum(peak_in[0], jnp.max(scores, axis=-1, keepdims=True))
        factor = jnp.exp(peak_in[0] - peak)
        weights = jnp.exp(scores - peak)
        peak_out[0] = peak
        sum_out[0] = sum_in[0] * factor + jnp.sum(weights, axis=-1, keepdims=True)
        acc_out[0] = acc_in[0] * factor + jnp.dot(
            weights.astype(jnp.bfloat16), v_ref[...], preferred_element_type=jnp.float32
        )

    @pl.when(valid_ref[0] <= 0)
    def _():
        peak_out[0] = peak_in[0]
        sum_out[0] = sum_in[0]
        acc_out[0] = acc_in[0]


def attend(q_heads, key_value, key_gates, query_gates, small_count, state, valid):
    heads, rows, width = q_heads.shape
    per_small = width // DS
    groups = key_value.shape[1] // (2 * width)
    block = rows // 3 if rows % 3 == 0 and (rows // 3) % 128 == 0 else rows
    diagonal = state is None
    small_groups = small_count // per_small

    def group(h):
        return jnp.where(h < small_count, h // per_small, h - small_count + small_groups)

    per_query = pl.BlockSpec((1, block, 1), lambda h, i: (h, i, 0))
    wide = pl.BlockSpec((1, block, width), lambda h, i: (h, i, 0))
    in_specs = [
        wide,
        pl.BlockSpec((rows, width), lambda h, i: (0, group(h))),
        pl.BlockSpec((rows, width), lambda h, i: (0, groups + group(h))),
        pl.BlockSpec((1, 1, rows), lambda h, i: (h, 0, 0)),
        per_query,
    ]
    operands = [q_heads, key_value, key_value, key_gates[:, None, :], query_gates[:, :, None]]
    aliases = {}
    if not diagonal:
        in_specs = [pl.BlockSpec(memory_space=pltpu.SMEM)] + in_specs + [per_query, per_query, wide]
        operands = [valid] + operands + list(state)
        aliases = {6: 0, 7: 1, 8: 2}
    column = jax.ShapeDtypeStruct((heads, rows, 1), jnp.float32)

    def kernel(*refs):
        attend_body(small_count, diagonal, *refs)

    return pl.pallas_call(
        kernel,
        grid=(heads, rows // block),
        in_specs=in_specs,
        out_specs=[per_query, per_query, wide],
        out_shape=[column, column, jax.ShapeDtypeStruct((heads, rows, width), jnp.float32)],
        input_output_aliases=aliases,
        cost_estimate=pl.CostEstimate(
            flops=heads * rows * rows * width * 4,
            bytes_accessed=heads * rows * width * 12,
            transcendentals=heads * rows * rows,
        ),
        compiler_params=pltpu.CompilerParams(
            dimension_semantics=("arbitrary", "arbitrary"), vmem_limit_bytes=56 * 1024 * 1024
        ),
    )(*operands)


def per_device(
    query_small,
    key_small,
    value_small,
    gates_small,
    query_large,
    key_large,
    value_large,
    gates_large,
    residual,
    mixer_small,
    mixer_large,
    mix_gain,
    value_weight,
    gate_weight,
    value_taps,
    gate_taps,
    down_weight,
    final_gain,
):
    shard_rows = query_small.shape[0]
    sp_index = lax.axis_index("sp")
    tp_index = lax.axis_index("tp")
    tensor_parts = lax.axis_size("tp")
    sp_count = lax.axis_size("sp")
    splits = all(
        count % 2 == 0 and count * size % (2 * DL) == 0
        for count, size in ((gates_small.shape[1], DS), (gates_large.shape[1], DL))
    )
    team = 2 if splits and sp_count % 2 == 0 else 1
    pair_count = sp_count // team
    pair, side = sp_index // team, sp_index % team
    half_small = query_small.shape[1] // team
    small_count = gates_small.shape[1] // team
    large_count = gates_large.shape[1] // team

    def half(array, which):
        width = array.shape[1] // team
        return lax.dynamic_slice_in_dim(array, which * width, width, 1)

    def halves(parts, which):
        return jnp.concatenate([half(a, which) for a in parts], axis=1)

    def exchanged(parts):
        if team == 1:
            return jnp.concatenate(parts, axis=1)
        return in_order(halves(parts, side), swapped(halves(parts, 1 - side), "sp"), 0)

    def in_order(own, other, axis):
        return jnp.where(
            side == 0,
            jnp.concatenate([own, other], axis=axis),
            jnp.concatenate([other, own], axis=axis),
        )

    gate_parts = (gates_small, gates_large)
    key_value = exchanged((key_small, key_large, value_small, value_large))
    if team == 1:
        own_gates = jnp.concatenate(gate_parts, axis=1).T
    else:
        own_gates = in_order(
            halves(gate_parts, side).T, swapped(halves(gate_parts, 1 - side).T, "sp"), 1
        )
    queries = exchanged((query_small, query_large))

    width = DL
    per_small = width // DS
    lane_head = jnp.arange(width) // DS
    q_heads = []
    for h in range(small_count):
        columns = queries[:, (h // per_small) * width : (h // per_small + 1) * width]
        q_heads.append(jnp.where(lane_head == h % per_small, columns, 0).astype(jnp.bfloat16))
    for h in range(large_count):
        q_heads.append(queries[:, half_small + h * width : half_small + (h + 1) * width])
    q_heads = jnp.stack(q_heads)

    mixers = jnp.concatenate([mixer_small, mixer_large], axis=0)
    mixer_of = [mixers]
    for s in range(1, tensor_parts):
        mixer_of.append(rotated(mixers, "tp", -s))
    full_value = lax.all_gather(value_weight, "sp", axis=0, tiled=True)
    full_gate = lax.all_gather(gate_weight, "sp", axis=0, tiled=True)
    down_pieces = down_parts(down_weight)

    arriving, gates_arriving = [key_value], [own_gates]
    for step in range(1, pair_count):
        gates_arriving.append(passed_along(own_gates, "sp", step * team))
        arriving.append(passed_along(arriving[-1], "sp", team))
    state = attend(q_heads, key_value, own_gates, own_gates, small_count, None, None)
    for step in range(1, pair_count):
        valid = (pair >= step).astype(jnp.int32).reshape(1)
        state = attend(
            q_heads, arriving[step], gates_arriving[step], own_gates, small_count, state, valid
        )
    head_out = (state[2] / state[1]).astype(jnp.bfloat16)
    columns = []
    for g in range(small_count // per_small):
        merged = head_out[g * per_small]
        for h in range(1, per_small):
            merged = jnp.where(lane_head == h, head_out[g * per_small + h], merged)
        columns.append(merged)
    for h in range(large_count):
        columns.append(head_out[small_count + h])
    attended = jnp.concatenate(columns, axis=1)
    joined = attended
    if team == 2:
        own = lax.dynamic_slice_in_dim(attended, side * shard_rows, shard_rows, 0)
        other = swapped(
            lax.dynamic_slice_in_dim(attended, (1 - side) * shard_rows, shard_rows, 0), "sp"
        )
        joined = jnp.concatenate(
            [
                in_order(own[:, :half_small], other[:, :half_small], 1),
                in_order(own[:, half_small:], other[:, half_small:], 1),
            ],
            axis=1,
        )
    own_rows = shard_rows // tensor_parts
    arrived = lax.all_to_all(joined, "tp", split_axis=0, concat_axis=1, tiled=True)
    mix = jnp.zeros((own_rows, mixers.shape[1]), jnp.float32)
    for s in range(tensor_parts):
        source = (tp_index + s) % tensor_parts
        mix = mix + jnp.dot(
            lax.dynamic_slice_in_dim(arrived, source * joined.shape[1], joined.shape[1], 1),
            mixer_of[s],
            preferred_element_type=jnp.float32,
        )
    mixed = norm_rows(residual_scale * residual.astype(jnp.float32) + mix, mix_gain).astype(
        jnp.bfloat16
    )
    block_input = jnp.zeros((shard_rows, mixed.shape[1]), jnp.bfloat16)
    for s in range(tensor_parts):
        piece = mixed if s == 0 else rotated(mixed, "tp", -s)
        source = (tp_index + s) % tensor_parts
        block_input = lax.dynamic_update_slice_in_dim(block_input, piece, source * own_rows, 0)

    up_value = jnp.dot(block_input, full_value, preferred_element_type=jnp.float32).astype(
        jnp.bfloat16
    )
    up_gate = jnp.dot(block_input, full_gate, preferred_element_type=jnp.float32).astype(
        jnp.bfloat16
    )
    down_base, up_value = lax.optimization_barrier((down_weight, up_value))
    full_down = assembled(down_base, down_pieces)
    hidden_width = up_value.shape[1]
    trailing = jnp.concatenate([up_value[-2:], up_gate[-2:]], axis=1)
    earlier = passed_along(trailing, "sp", 1)
    padded_value = jnp.concatenate([earlier[:, :hidden_width], up_value], axis=0).astype(
        jnp.float32
    )
    padded_gate = jnp.concatenate([earlier[:, hidden_width:], up_gate], axis=0).astype(jnp.float32)
    filt_value = (
        value_taps[0] * padded_value[:-2]
        + value_taps[1] * padded_value[1:-1]
        + value_taps[2] * padded_value[2:]
    )
    filt_gate = (
        gate_taps[0] * padded_gate[:-2]
        + gate_taps[1] * padded_gate[1:-1]
        + gate_taps[2] * padded_gate[2:]
    )
    hidden = (jax.nn.silu(filt_gate) * filt_value).astype(jnp.bfloat16)

    def ffn_rows(s):
        target = (tp_index + s) % tensor_parts
        part = lax.dynamic_slice_in_dim(hidden, target * own_rows, own_rows, 0)
        return jnp.dot(part, full_down, preferred_element_type=jnp.float32)

    order = [tensor_parts // 2] + [s for s in range(1, tensor_parts) if s != tensor_parts // 2]
    received = [rotated(ffn_rows(s).astype(jnp.bfloat16), "tp", s) for s in order]
    ffn = ffn_rows(0)
    for part in received:
        ffn = ffn + part.astype(jnp.float32)
    return norm_rows(residual_scale * mixed.astype(jnp.float32) + ffn, final_gain).astype(
        jnp.bfloat16
    )


def down_parts(down_weight):
    pieces = []
    for s in range(1, lax.axis_size("sp")):
        pieces.append(rotated(down_weight, "sp", -s))
    return pieces


def assembled(own, pieces):
    count = lax.axis_size("sp")
    width = own.shape[1]
    index = lax.axis_index("sp")
    full = jnp.zeros((own.shape[0], count * width), own.dtype)
    for s, piece in enumerate([own] + pieces):
        full = lax.dynamic_update_slice_in_dim(full, piece, ((index + s) % count) * width, 1)
    return full


def solution(mesh):
    in_specs = (
        P("sp", "tp"),
        P("sp", "tp"),
        P("sp", "tp"),
        P("sp", "tp"),
        P("sp", "tp"),
        P("sp", "tp"),
        P("sp", "tp"),
        P("sp", "tp"),
        P(("sp", "tp"), None),
        P("tp", None),
        P("tp", None),
        P(),
        P("sp", "tp"),
        P("sp", "tp"),
        P(None, "tp"),
        P(None, "tp"),
        P("tp", "sp"),
        P(),
    )
    out_specs = P(("sp", "tp"), None)

    return jax.shard_map(
        per_device, mesh=mesh, in_specs=in_specs, out_specs=out_specs, check_vma=False
    )
```

time: 714 us -> 578 us (0.81); the launches traced: 713 us -> 567 us
  waiting for transfers between devices: 527 us -> 260 us
  starting transfers between devices: 2.86 us -> 146 us
  blocking collectives: 83.4 us -> 0 us
  Pallas kernels: 0 us -> 55.5 us
  matrix products: 53.3 us -> 31.5 us
  local copies, waits for them, and re-layouts: 14 us -> 30.6 us
  other arithmetic: 17.8 us -> 28.6 us
    all_gather x10 -> x2, waiting for transfers between devices: 486 us -> 0.02 us  [the longest x1 0.02 us: per_device(): full_value = lax.all_gather(value_weight, 'sp', axis=0, tiled=True)]
    ppermute x1 -> x7, waiting for transfers between devices: 1.43 us -> 110 us  [passed_along(): lax.ppermute(value, axis, [(source, source + steps) for source in range(f...]
    ppermute x0 -> x20, waiting for transfers between devices: none -> 85.7 us  [the longest x16 52 us: rotated(): lax.ppermute(value, axis, [(s, (s + steps) % count) for s in range(count)])]
    ppermute x1 -> x7, starting transfers between devices: 2.46 us -> 84.7 us  [passed_along(): lax.ppermute(value, axis, [(source, source + steps) for source in range(f...]
    all_gather x2 -> x0, blocking collectives: 64.4 us -> none  [the longest x1 33.1 us: per_device(): lax.all_gather(gates_large, 'sp', axis=0, tiled=True)]
    all_to_all x0 -> x1, waiting for transfers between devices: none -> 63.6 us  [per_device(): lax.all_to_all(joined, 'tp', split_axis=0, concat_axis=1, tiled=True)]
    ppermute x0 -> x20, starting transfers between devices: none -> 58.1 us  [the longest x16 51.8 us: rotated(): lax.ppermute(value, axis, [(s, (s + steps) % count) for s in range(count)])]
    pallas_call x0 -> x4, Pallas kernels: none -> 55.5 us  [attend(): pl.pallas_call(kernel, grid=(heads, rows // block), in_specs=in_specs, ou...]
  transfers between devices with their start and end apart: 12 -> 30, of which waited for: 10 -> 11; matrix products, arithmetic and copies ran while one was open for 8% -> 13% of each run, Pallas kernels for 0% -> 10%
where the time goes in v1:
time: 578 us; the launch traced here: 567 us
  waiting for transfers between devices  260 us (45%)
  starting transfers between devices  146 us (25%)
  Pallas kernels  55.5 us (10%)
  matrix products  31.5 us (5%)
  local copies, waits for them, and re-layouts  30.6 us (5%)
  other arithmetic  28.6 us (5%)
  between operations  14.1 us (2%)
    ppermute x7, waiting for transfers between devices, passed_along(): lax.ppermute(value, axis, [(source, source + steps) for source in range(f...  110 us
    ppermute x7, starting transfers between devices, passed_along(): lax.ppermute(value, axis, [(source, source + steps) for source in range(f...  84.7 us
    all_to_all x1, waiting for transfers between devices, per_device(): lax.all_to_all(joined, 'tp', split_axis=0, concat_axis=1, tiled=True)  63.6 us
    pallas_call x4, Pallas kernels, attend(): pl.pallas_call(kernel, grid=(heads, rows // block), in_specs=in_specs, ou...  55.5 us
    ppermute x16, waiting for transfers between devices, rotated(): lax.ppermute(value, axis, [(s, (s + steps) % count) for s in range(count)])  52 us
    ppermute x16, starting transfers between devices, rotated(): lax.ppermute(value, axis, [(s, (s + steps) % count) for s in range(count)])  51.8 us
    ppermute x4, waiting for transfers between devices, swapped(): lax.ppermute(value, axis, [(s, s ^ 1) for s in range(lax.axis_size(axis))])  33.7 us
    select_n x7, other arithmetic, in_order(): jnp.where(side == 0, jnp.concatenate([own, other], axis=axis), jnp.concat...  12.2 us
  transfers between devices with their start and end apart: 30, of which 11 were waited for; matrix products, arithmetic and copies ran while one was open for 13% of the time, Pallas kernels for 10%

profile of v1, /device:TPU:0, one launch (start us, length us, event | category | flops | bytes accessed | tf_op | source)
XLA Modules:
  0.0 567.1 jit_solution(7286071290898381385)
XLA Ops:
  7.3 1.3 constant_dynamic-slice_fusion.10
  9.6 3.0 collective-permute-start.1
  12.6 25.3 %collective-permute-done.1 = bf16[768,512]{1,0:T(8,128)(2,1)S(1)} collective-permute-done((bf16[768,512]{1,0:T(8,128)(2,1)S(1)}, bf16[768,512]{1,0:T(8,128)(2,1)S(1)}, u32[]{:S(2)}, u32[]{:S(2)}) %collective-permute-start.1) | collective-permute-done | bytes 786464 | tf_op jit(solution)/shard_map/ppermute | solution.py:29
  37.9 5.0 maximum_select_fusion.1.refs_1_.refs_2_
  42.9 3.8 collective-permute-start.2
  46.8 1.3 constant_dynamic-slice_fusion.14
  48.9 1.5 collective-permute-start
  52.9 1.4 fusion.32
  54.3 54.4 %collective-permute-done.2.refs_2_.refs_3_ = bf16[1536,512]{1,0:T(8,128)(2,1)S(1)} collective-permute-done((bf16[1536,512]{1,0:T(8,128)(2,1)S(1)}, bf16[1536,512]{1,0:T(8,128)(2,1)S(1)}, u32[]{:S(2)}, u32[]{:S(2)}) %collective-permute-start.2) | collective-permute-done | bytes 1572896 | tf_op jit(solution)/shard_map/ppermute | solution.py:20
  108.7 23.0 %collective-permute-start.3 = (bf16[1536,512]{1,0:T(8,128)(2,1)S(1)}, bf16[1536,512]{1,0:T(8,128)(2,1)S(1)}, u32[]{:S(2)}, u32[]{:S(2)}) collective-permute-start(bf16[1536,512]{1,0:T(8,128)(2,1)S(1)} %collective-permute-done.2.refs_2_.refs_3_), channel_id=1, source_target_pairs={{0,8},{4,12},{8,16},{12,20},{16,24},{20,28},{1,9},{5,13},{9,17},{1... | collective-permute-start | bytes 4718600 | tf_op jit(solution)/shard_map/ppermute | solution.py:20
  131.7 2.3 constant_dynamic-update-slice_fusion.13
  135.7 2.1 copy.57
  137.9 1.4 maximum_select_fusion.5
  139.2 4.9 collective-permute-start.8
  144.1 3.0 collective-permute-start.7
  147.1 1.9 collective-permute-start.6
  149.0 1.4 copy.58
  150.4 4.1 maximum_select_fusion.refs_4_.refs_5_
  155.1 34.0 %collective-permute-done.8 = f32[3,1536]{1,0:T(4,128)} collective-permute-done((f32[3,1536]{1,0:T(4,128)}, f32[3,1536]{1,0:T(4,128)}, u32[]{:S(2)}, u32[]{:S(2)}) %collective-permute-start.8) | collective-permute-done | bytes 18464 | tf_op jit(solution)/shard_map/ppermute | solution.py:20
  189.1 1.4 copy.62.refs_4_
  190.4 1.4 copy.63.refs_4_
  191.8 1.3 broadcast_in_dim.45.refs_4_
  193.1 1.4 maximum_select_fusion.2
  194.6 5.4 collective-permute-start.4
  201.2 24.2 %shard_map.172 = (f32[3,1536,1]{2,1,0:T(8,128)}, f32[3,1536,1]{2,1,0:T(8,128)}, f32[3,1536,128]{2,1,0:T(8,128)}) custom-call(bf16[3,1536,128]{2,1,0:T(8,128)(2,1)} %pad_maximum_fusion.refs_0_.refs_1_, bf16[1536,512]{1,0:T(8,128)(2,1)} %copy-done.5, bf16[1536,512]{1,0:T(8,128)(2,1)} %copy-done.5, f32[3,1,1536]{2,1,0:T(1,128)} %copy.61.refs_3_, ...), custom_call_target="tpu_custom_call" | custom-call | flops 3623878656 | bytes 7077888 | tf_op jit(solution)/shard_map/pallas_call | solution.py:119
  225.4 10.5 %shard_map.173 = (f32[3,1536,1]{2,1,0:T(8,128)}, f32[3,1536,1]{2,1,0:T(8,128)}, f32[3,1536,128]{2,1,0:T(8,128)}) custom-call(s32[1]{0:T(128)} %bitcast.11.refs_0_, bf16[3,1536,128]{2,1,0:T(8,128)(2,1)} %pad_maximum_fusion.refs_0_.refs_1_, bf16[1536,512]{1,0:T(8,128)(2,1)} %copy-done.1, ...), custom_call_target="tpu_custom_call", output_to_operand_aliasing={{0}: (6, {}), {1}: (7, {}), {2}: (8, {})} | custom-call | flops 3623878656 | bytes 7077888 | tf_op jit(solution)/shard_map/pallas_call | solution.py:119
  235.9 10.4 %shard_map.174 = (f32[3,1536,1]{2,1,0:T(8,128)}, f32[3,1536,1]{2,1,0:T(8,128)}, f32[3,1536,128]{2,1,0:T(8,128)}) custom-call(s32[1]{0:T(128)} %bitcast.9.refs_0_, bf16[3,1536,128]{2,1,0:T(8,128)(2,1)} %pad_maximum_fusion.refs_0_.refs_1_, bf16[1536,512]{1,0:T(8,128)(2,1)} %copy-done.2, ...), custom_call_target="tpu_custom_call", output_to_operand_aliasing={{0}: (6, {}), {1}: (7, {}), {2}: (8, {})} | custom-call | flops 3623878656 | bytes 7077888 | tf_op jit(solution)/shard_map/pallas_call | solution.py:119
  246.3 21.8 %collective-permute-done.4.refs_2_.refs_3_ = bf16[1536,512]{1,0:T(8,128)(2,1)S(1)} collective-permute-done((bf16[1536,512]{1,0:T(8,128)(2,1)S(1)}, bf16[1536,512]{1,0:T(8,128)(2,1)S(1)}, u32[]{:S(2)}, u32[]{:S(2)}) %collective-permute-start.4) | collective-permute-done | bytes 1572896 | tf_op jit(solution)/shard_map/ppermute | solution.py:20
  269.3 10.4 %shard_map.175 = (f32[3,1536,1]{2,1,0:T(8,128)}, f32[3,1536,1]{2,1,0:T(8,128)}, f32[3,1536,128]{2,1,0:T(8,128)}) custom-call(s32[1]{0:T(128)} %bitcast.refs_0_, bf16[3,1536,128]{2,1,0:T(8,128)(2,1)} %pad_maximum_fusion.refs_0_.refs_1_, bf16[1536,512]{1,0:T(8,128)(2,1)} %copy-done.3, ...), custom_call_target="tpu_custom_call", output_to_operand_aliasing={{0}: (6, {}), {1}: (7, {}), {2}: (8, {})} | custom-call | flops 3623878656 | bytes 7077888 | tf_op jit(solution)/shard_map/pallas_call | solution.py:119
  279.7 2.5 reduce
  283.2 1.2 collective-permute-start.9
  285.1 1.3 collective-permute-start.11
  286.5 8.4 %collective-permute-done.9 = bf16[768,256]{1,0:T(8,128)(2,1)S(1)} collective-permute-done((bf16[768,256]{1,0:T(8,128)(2,1)S(1)}, bf16[768,256]{1,0:T(8,128)(2,1)S(1)}, u32[]{:S(2)}, u32[]{:S(2)}) %collective-permute-start.9) | collective-permute-done | bytes 393248 | tf_op jit(solution)/shard_map/ppermute | solution.py:29
  296.1 3.7 all-to-all-start
  299.9 63.6 %all-to-all-done = bf16[4,192,512]{2,1,0:T(8,128)(2,1)S(1)} async-done(((bf16[4,192,512]{2,1,0:T(8,128)(2,1)}), bf16[4,192,512]{2,1,0:T(8,128)(2,1)S(1)}, u32[]{:S(2)}, u32[]{:S(2)}) %all-to-all-start) | async-done | bytes 786464 | tf_op jit(solution)/shard_map/all_to_all | solution.py:255
  363.7 2.2 fusion.22
  365.9 2.2 fusion.18
  369.2 2.5 fusion.38
  372.5 1.2 constant_dynamic-update-slice_fusion.11
  375.1 18.8 %collective-permute-start.17 = (bf16[1408,256]{1,0:T(8,128)(2,1)}, bf16[1408,256]{1,0:T(8,128)(2,1)}, u32[]{:S(2)}, u32[]{:S(2)}) collective-permute-start(bf16[1408,256]{1,0:T(8,128)(2,1)} %param.34), channel_id=1, source_target_pairs={{0,28},{4,0},{8,4},{12,8},{16,12},{20,16},{24,20},{28,24},{1,29},{... | collective-permute-start | bytes 2162696 | tf_op jit(solution)/shard_map/ppermute | solution.py:25
  394.0 5.4 collective-permute-start.19
  399.4 1.2 constant_dynamic-update-slice_fusion.10
  400.6 9.4 %collective-permute-done.14 = bf16[192,2048]{1,0:T(8,128)(2,1)} collective-permute-done((bf16[192,2048]{1,0:T(8,128)(2,1)}, bf16[192,2048]{1,0:T(8,128)(2,1)}, u32[]{:S(2)}, u32[]{:S(2)}) %collective-permute-start.14) | collective-permute-done | bytes 786464 | tf_op jit(solution)/shard_map/ppermute | solution.py:25
  410.0 9.3 %collective-permute-start.20 = (bf16[1408,256]{1,0:T(8,128)(2,1)}, bf16[1408,256]{1,0:T(8,128)(2,1)}, u32[]{:S(2)}, u32[]{:S(2)}) collective-permute-start(bf16[1408,256]{1,0:T(8,128)(2,1)} %param.34), channel_id=1, source_target_pairs={{0,16},{4,20},{8,24},{12,28},{16,0},{20,4},{24,8},{28,12},{1,17},{... | collective-permute-start | bytes 2162696 | tf_op jit(solution)/shard_map/ppermute | solution.py:25
  419.3 1.2 constant_dynamic-update-slice_fusion.9
  420.5 10.4 %collective-permute-start.21 = (bf16[1408,256]{1,0:T(8,128)(2,1)}, bf16[1408,256]{1,0:T(8,128)(2,1)}, u32[]{:S(2)}, u32[]{:S(2)}) collective-permute-start(bf16[1408,256]{1,0:T(8,128)(2,1)} %param.34), channel_id=1, source_target_pairs={{0,12},{4,16},{8,20},{12,24},{16,28},{20,0},{24,4},{28,8},{1,13},{... | collective-permute-start | bytes 2162696 | tf_op jit(solution)/shard_map/ppermute | solution.py:25
  431.0 1.2 constant_dynamic-update-slice_fusion.8
  432.2 8.8 %convolution_convert_fusion.1 = bf16[768,1408]{1,0:T(8,128)(2,1)} fusion(bf16[768,2048]{1,0:T(8,128)(2,1)S(1)} %constant_dynamic-update-slice_fusion.8, bf16[2048,1408]{1,0:T(8,128)(2,1)} %all-gather.3.cloned.1.call-done), kind=kOutput, calls=%fused_computation.13 | convolution fusion | flops 4430266368 | bytes 11075584 | tf_op jit(solution)/shard_map/dot_general | solution.py:273
  441.0 8.0 %convolution_convert_fusion = bf16[768,1408]{1,0:T(8,128)(2,1)S(1)} fusion(bf16[768,2048]{1,0:T(8,128)(2,1)S(1)} %constant_dynamic-update-slice_fusion.8, bf16[2048,1408]{1,0:T(8,128)(2,1)} %all-gather.5.cloned.1.call-done), kind=kOutput, calls=%fused_computation.12 | convolution fusion | flops 4430266368 | bytes 11075584 | tf_op jit(solution)/shard_map/dot_general | solution.py:276
  449.8 1.2 constant_dynamic-update-slice_fusion.7
  452.4 1.5 collective-permute-start.23
  455.1 42.7 %collective-permute-start.16 = (bf16[2,2816]{1,0:T(2,128)(2,1)S(1)}, bf16[2,2816]{1,0:T(2,128)(2,1)S(1)}, u32[]{:S(2)}, u32[]{:S(2)}) collective-permute-start(bf16[2,2816]{1,0:T(2,128)(2,1)S(1)} %pad_maximum_fusion.5), channel_id=1, source_target_pairs={{0,4},{4,8},{8,12},{12,16},{16,20},{20,24},{24,28},{1,5},{5,9},{9,... | collective-permute-start | bytes 33800 | tf_op jit(solution)/shard_map/ppermute | solution.py:20
  497.8 1.2 constant_dynamic-update-slice_fusion.4
  499.0 10.4 %collective-permute-done.20 = bf16[1408,256]{1,0:T(8,128)(2,1)} collective-permute-done((bf16[1408,256]{1,0:T(8,128)(2,1)}, bf16[1408,256]{1,0:T(8,128)(2,1)}, u32[]{:S(2)}, u32[]{:S(2)}) %collective-permute-start.20) | collective-permute-done | bytes 720928 | tf_op jit(solution)/shard_map/ppermute | solution.py:25
  509.4 1.2 constant_dynamic-update-slice_fusion.3
  510.8 1.2 constant_dynamic-update-slice_fusion.2
  513.1 3.5 fusion.2
  516.7 1.4 convolution_convert_fusion.4
  518.1 1.4 convolution_convert_fusion.3
  519.5 1.4 convolution_convert_fusion.2
  522.0 1.7 collective-permute-start.26
  523.8 17.6 %collective-permute-done.24 = bf16[192,2048]{1,0:T(8,128)(2,1)S(1)} collective-permute-done((bf16[192,2048]{1,0:T(8,128)(2,1)S(1)}, bf16[192,2048]{1,0:T(8,128)(2,1)S(1)}, u32[]{:S(2)}, u32[]{:S(2)}) %collective-permute-start.24) | collective-permute-done | bytes 786464 | tf_op jit(solution)/shard_map/ppermute | solution.py:25
  541.4 14.4 %collective-permute-done.25 = bf16[192,2048]{1,0:T(8,128)(2,1)S(1)} collective-permute-done((bf16[192,2048]{1,0:T(8,128)(2,1)S(1)}, bf16[192,2048]{1,0:T(8,128)(2,1)S(1)}, u32[]{:S(2)}, u32[]{:S(2)}) %collective-permute-start.25) | collective-permute-done | bytes 786464 | tf_op jit(solution)/shard_map/ppermute | solution.py:25
  555.7 2.9 fusion.39
  (111 shorter events, 23.2 us)
Async XLA Ops:
  6.5 2.1 copy-start.9
  6.5 2.1 copy-start.8
  6.5 425.7 %all-gather.3.cloned.1.call-start = ((), (), s32[]{:S(2)}) async-start(), calls=%async_computation.1 | async-start | bytes 6488064 | tf_op jit(solution)/shard_map/all_gather | solution.py:217
  7.3 433.8 %all-gather.5.cloned.1.call-start = ((), (), s32[]{:S(2)}) async-start(), calls=%async_computation.2 | async-start | bytes 6488064 | tf_op jit(solution)/shard_map/all_gather | solution.py:218
  9.6 28.3 %collective-permute-start.1 = (bf16[768,512]{1,0:T(8,128)(2,1)S(1)}, bf16[768,512]{1,0:T(8,128)(2,1)S(1)}, u32[]{:S(2)}, u32[]{:S(2)}) collective-permute-start(bf16[768,512]{1,0:T(8,128)(2,1)S(1)} %pad_maximum_fusion.1), channel_id=1, source_target_pairs={{0,4},{4,0},{8,12},{12,8},{16,20},{20,16},{24,28},{28,24},{1,5},{5... | collective-permute-start | bytes 2359304 | tf_op jit(solution)/shard_map/ppermute | solution.py:29
  37.9 13.2 %copy-start.13 = (f32[768,4]{0,1:T(4,128)S(1)}, f32[768,4]{0,1:T(4,128)}, u32[]{:S(2)}) copy-start(f32[768,4]{0,1:T(4,128)} %param.21) | copy-start | bytes 36868
  42.9 11.4 %copy-start.5 = (bf16[1536,512]{1,0:T(8,128)(2,1)}, bf16[1536,512]{1,0:T(8,128)(2,1)S(1)}, u32[]{:S(2)}) copy-start(bf16[1536,512]{1,0:T(8,128)(2,1)S(1)} %maximum_select_fusion.1.refs_1_.refs_2_) | copy-start | bytes 4718596
  42.9 65.8 %collective-permute-start.2 = (bf16[1536,512]{1,0:T(8,128)(2,1)S(1)}, bf16[1536,512]{1,0:T(8,128)(2,1)S(1)}, u32[]{:S(2)}, u32[]{:S(2)}) collective-permute-start(bf16[1536,512]{1,0:T(8,128)(2,1)S(1)} %maximum_select_fusion.1.refs_1_.refs_2_), channel_id=1, source_target_pairs={{0,8},{4,12},{8,16},{12,20},{16,24},{20,28},{1,9},{5,13},{9,17},{1... | collective-permute-start | bytes 4718600 | tf_op jit(solution)/shard_map/ppermute | solution.py:20
  48.9 144.3 %collective-permute-start = (bf16[768,256]{1,0:T(8,128)(2,1)}, bf16[768,256]{1,0:T(8,128)(2,1)}, u32[]{:S(2)}, u32[]{:S(2)}) collective-permute-start(bf16[768,256]{1,0:T(8,128)(2,1)} %pad_maximum_fusion.3), channel_id=1, source_target_pairs={{0,4},{4,0},{8,12},{12,8},{16,20},{20,16},{24,28},{28,24},{1,5},{5... | collective-permute-start | bytes 1179656 | tf_op jit(solution)/shard_map/ppermute | solution.py:29
  52.4 85.5 %collective-permute-start.5 = (f32[3,768]{1,0:T(4,128)}, f32[3,768]{1,0:T(4,128)S(1)}, u32[]{:S(2)}, u32[]{:S(2)}) collective-permute-start(f32[3,768]{1,0:T(4,128)} %maximum_bitcast_fusion), channel_id=1, source_target_pairs={{0,4},{4,0},{8,12},{12,8},{16,20},{20,16},{24,28},{28,24},{1,5},{5... | collective-permute-start | bytes 27656 | tf_op jit(solution)/shard_map/ppermute | solution.py:29
  52.9 81.1 %copy-start.6 = (bf16[256,2048]{1,0:T(8,128)(2,1)S(1)}, bf16[256,2048]{1,0:T(8,128)(2,1)}, u32[]{:S(2)}) copy-start(bf16[256,2048]{1,0:T(8,128)(2,1)} %param.28) | copy-start | bytes 3145732
  108.7 29.2 %copy-start.1 = (bf16[1536,512]{1,0:T(8,128)(2,1)}, bf16[1536,512]{1,0:T(8,128)(2,1)S(1)}, u32[]{:S(2)}) copy-start(bf16[1536,512]{1,0:T(8,128)(2,1)S(1)} %collective-permute-done.2.refs_2_.refs_3_) | copy-start | bytes 4718596
  108.7 85.9 %collective-permute-start.3 = (bf16[1536,512]{1,0:T(8,128)(2,1)S(1)}, bf16[1536,512]{1,0:T(8,128)(2,1)S(1)}, u32[]{:S(2)}, u32[]{:S(2)}) collective-permute-start(bf16[1536,512]{1,0:T(8,128)(2,1)S(1)} %collective-permute-done.2.refs_2_.refs_3_), channel_id=1, source_target_pairs={{0,8},{4,12},{8,16},{12,20},{16,24},{20,28},{1,9},{5,13},{9,17},{1... | collective-permute-start | bytes 4718600 | tf_op jit(solution)/shard_map/ppermute | solution.py:20
  139.2 49.8 %collective-permute-start.8 = (f32[3,1536]{1,0:T(4,128)}, f32[3,1536]{1,0:T(4,128)}, u32[]{:S(2)}, u32[]{:S(2)}) collective-permute-start(f32[3,1536]{1,0:T(4,128)} %maximum_select_fusion.5), channel_id=1, source_target_pairs={{0,8},{4,12},{8,16},{12,20},{16,24},{20,28},{1,9},{5,13},{9,17},{1... | collective-permute-start | bytes 55304 | tf_op jit(solution)/shard_map/ppermute | solution.py:20
  144.1 46.3 %collective-permute-start.7 = (f32[3,1536]{1,0:T(4,128)}, f32[3,1536]{1,0:T(4,128)}, u32[]{:S(2)}, u32[]{:S(2)}) collective-permute-start(f32[3,1536]{1,0:T(4,128)} %maximum_select_fusion.5), channel_id=1, source_target_pairs={{0,16},{4,20},{8,24},{12,28},{1,17},{5,21},{9,25},{13,29},{2,18},{... | collective-permute-start | bytes 55304 | tf_op jit(solution)/shard_map/ppermute | solution.py:20
  147.1 44.7 %collective-permute-start.6 = (f32[3,1536]{1,0:T(4,128)}, f32[3,1536]{1,0:T(4,128)}, u32[]{:S(2)}, u32[]{:S(2)}) collective-permute-start(f32[3,1536]{1,0:T(4,128)} %maximum_select_fusion.5), channel_id=1, source_target_pairs={{0,24},{4,28},{1,25},{5,29},{2,26},{6,30},{3,27},{7,31}} | collective-permute-start | bytes 55304 | tf_op jit(solution)/shard_map/ppermute | solution.py:20
  150.4 4.1 copy-start.10
  150.4 49.6 %copy-start.16 = (pred[128]{0:T(512)(128)(4,1)S(1)}, pred[128]{0:T(512)(128)(4,1)}, u32[]{:S(2)}) copy-start(pred[128]{0:T(512)(128)(4,1)} %get-tuple-element.73) | copy-start | bytes 388
  189.1 176.8 %collective-permute-start.12 = (bf16[512,2048]{1,0:T(8,128)(2,1)}, bf16[512,2048]{1,0:T(8,128)(2,1)}, u32[]{:S(2)}, u32[]{:S(2)}) collective-permute-start(bf16[512,2048]{1,0:T(8,128)(2,1)} %constant_dynamic-update-slice_fusion.12), channel_id=1, source_target_pairs={{0,1},{1,2},{2,3},{3,0},{4,5},{5,6},{6,7},{7,4},{8,9},{9,10},{10,1... | collective-permute-start | bytes 6291464 | tf_op jit(solution)/shard_map/ppermute | solution.py:25
  194.6 30.8 %copy-start.2 = (bf16[1536,512]{1,0:T(8,128)(2,1)}, bf16[1536,512]{1,0:T(8,128)(2,1)S(1)}, u32[]{:S(2)}) copy-start(bf16[1536,512]{1,0:T(8,128)(2,1)S(1)} %collective-permute-done.3.refs_2_.refs_3_) | copy-start | bytes 4718596
  194.6 73.5 %collective-permute-start.4 = (bf16[1536,512]{1,0:T(8,128)(2,1)S(1)}, bf16[1536,512]{1,0:T(8,128)(2,1)S(1)}, u32[]{:S(2)}, u32[]{:S(2)}) collective-permute-start(bf16[1536,512]{1,0:T(8,128)(2,1)S(1)} %collective-permute-done.3.refs_2_.refs_3_), channel_id=1, source_target_pairs={{0,8},{4,12},{8,16},{12,20},{16,24},{20,28},{1,9},{5,13},{9,17},{1... | collective-permute-start | bytes 4718600 | tf_op jit(solution)/shard_map/ppermute | solution.py:20
  268.1 1.2 copy-start.3
  279.7 2.5 copy-start
  283.2 11.7 %collective-permute-start.9 = (bf16[768,256]{1,0:T(8,128)(2,1)S(1)}, bf16[768,256]{1,0:T(8,128)(2,1)S(1)}, u32[]{:S(2)}, u32[]{:S(2)}) collective-permute-start(bf16[768,256]{1,0:T(8,128)(2,1)S(1)} %get-tuple-element.40), channel_id=1, source_target_pairs={{0,4},{4,0},{8,12},{12,8},{16,20},{20,16},{24,28},{28,24},{1,5},{5... | collective-permute-start | bytes 1179656 | tf_op jit(solution)/shard_map/ppermute | solution.py:29
  284.4 83.6 %collective-permute-start.10 = (bf16[512,2048]{1,0:T(8,128)(2,1)}, bf16[512,2048]{1,0:T(8,128)(2,1)S(1)}, u32[]{:S(2)}, u32[]{:S(2)}) collective-permute-start(bf16[512,2048]{1,0:T(8,128)(2,1)} %constant_dynamic-update-slice_fusion.12), channel_id=1, source_target_pairs={{0,3},{1,0},{2,1},{3,2},{4,7},{5,4},{6,5},{7,6},{8,11},{9,8},{10,9... | collective-permute-start | bytes 6291464 | tf_op jit(solution)/shard_map/ppermute | solution.py:25
  285.1 83.6 %collective-permute-start.11 = (bf16[512,2048]{1,0:T(8,128)(2,1)}, bf16[512,2048]{1,0:T(8,128)(2,1)}, u32[]{:S(2)}, u32[]{:S(2)}) collective-permute-start(bf16[512,2048]{1,0:T(8,128)(2,1)} %constant_dynamic-update-slice_fusion.12), channel_id=1, source_target_pairs={{0,2},{1,3},{2,0},{3,1},{4,6},{5,7},{6,4},{7,5},{8,10},{9,11},{10,... | collective-permute-start | bytes 6291464 | tf_op jit(solution)/shard_map/ppermute | solution.py:25
  296.1 67.4 %all-to-all-start = ((bf16[4,192,512]{2,1,0:T(8,128)(2,1)}), bf16[4,192,512]{2,1,0:T(8,128)(2,1)S(1)}, u32[]{:S(2)}, u32[]{:S(2)}) async-start(bf16[4,192,512]{2,1,0:T(8,128)(2,1)} %pad_maximum_fusion.2), calls=%async_computation | async-start | bytes 1572864 | tf_op jit(solution)/shard_map/all_to_all | solution.py:255
  368.1 1.1 copy-start.7
  371.7 0.7 copy-start.14
  372.5 21.4 %copy-start.11 = (f32[3,1408]{1,0:T(4,128)S(1)}, f32[3,1408]{1,0:T(4,128)}, u32[]{:S(2)}) copy-start(f32[3,1408]{1,0:T(4,128)} %param.32) | copy-start | bytes 50692
  372.5 21.4 %copy-start.12 = (f32[3,1408]{1,0:T(4,128)S(1)}, f32[3,1408]{1,0:T(4,128)}, u32[]{:S(2)}) copy-start(f32[3,1408]{1,0:T(4,128)} %param.33) | copy-start | bytes 50692
  373.7 20.3 %collective-permute-start.13 = (bf16[192,2048]{1,0:T(8,128)(2,1)}, bf16[192,2048]{1,0:T(8,128)(2,1)}, u32[]{:S(2)}, u32[]{:S(2)}) collective-permute-start(bf16[192,2048]{1,0:T(8,128)(2,1)} %get-tuple-element.38), channel_id=1, source_target_pairs={{0,3},{1,0},{2,1},{3,2},{4,7},{5,4},{6,5},{7,6},{8,11},{9,8},{10,9... | collective-permute-start | bytes 2359304 | tf_op jit(solution)/shard_map/ppermute | solution.py:25
  373.7 36.3 %collective-permute-start.14 = (bf16[192,2048]{1,0:T(8,128)(2,1)}, bf16[192,2048]{1,0:T(8,128)(2,1)}, u32[]{:S(2)}, u32[]{:S(2)}) collective-permute-start(bf16[192,2048]{1,0:T(8,128)(2,1)} %get-tuple-element.38), channel_id=1, source_target_pairs={{0,2},{1,3},{2,0},{3,1},{4,6},{5,7},{6,4},{7,5},{8,10},{9,11},{10,... | collective-permute-start | bytes 2359304 | tf_op jit(solution)/shard_map/ppermute | solution.py:25
  374.9 45.7 %collective-permute-start.15 = (bf16[192,2048]{1,0:T(8,128)(2,1)}, bf16[192,2048]{1,0:T(8,128)(2,1)}, u32[]{:S(2)}, u32[]{:S(2)}) collective-permute-start(bf16[192,2048]{1,0:T(8,128)(2,1)} %get-tuple-element.38), channel_id=1, source_target_pairs={{0,1},{1,2},{2,3},{3,0},{4,5},{5,6},{6,7},{7,4},{8,9},{9,10},{10,1... | collective-permute-start | bytes 2359304 | tf_op jit(solution)/shard_map/ppermute | solution.py:25
  375.1 76.0 %collective-permute-start.17 = (bf16[1408,256]{1,0:T(8,128)(2,1)}, bf16[1408,256]{1,0:T(8,128)(2,1)}, u32[]{:S(2)}, u32[]{:S(2)}) collective-permute-start(bf16[1408,256]{1,0:T(8,128)(2,1)} %param.34), channel_id=1, source_target_pairs={{0,28},{4,0},{8,4},{12,8},{16,12},{20,16},{24,20},{28,24},{1,29},{... | collective-permute-start | bytes 2162696 | tf_op jit(solution)/shard_map/ppermute | solution.py:25
  393.9 58.5 %collective-permute-start.18 = (bf16[1408,256]{1,0:T(8,128)(2,1)}, bf16[1408,256]{1,0:T(8,128)(2,1)}, u32[]{:S(2)}, u32[]{:S(2)}) collective-permute-start(bf16[1408,256]{1,0:T(8,128)(2,1)} %param.34), channel_id=1, source_target_pairs={{0,24},{4,28},{8,0},{12,4},{16,8},{20,12},{24,16},{28,20},{1,25},{... | collective-permute-start | bytes 2162696 | tf_op jit(solution)/shard_map/ppermute | solution.py:25
  394.0 61.0 %collective-permute-start.19 = (bf16[1408,256]{1,0:T(8,128)(2,1)}, bf16[1408,256]{1,0:T(8,128)(2,1)}, u32[]{:S(2)}, u32[]{:S(2)}) collective-permute-start(bf16[1408,256]{1,0:T(8,128)(2,1)} %param.34), channel_id=1, source_target_pairs={{0,20},{4,24},{8,28},{12,0},{16,4},{20,8},{24,12},{28,16},{1,21},{... | collective-permute-start | bytes 2162696 | tf_op jit(solution)/shard_map/ppermute | solution.py:25
  410.0 99.4 %collective-permute-start.20 = (bf16[1408,256]{1,0:T(8,128)(2,1)}, bf16[1408,256]{1,0:T(8,128)(2,1)}, u32[]{:S(2)}, u32[]{:S(2)}) collective-permute-start(bf16[1408,256]{1,0:T(8,128)(2,1)} %param.34), channel_id=1, source_target_pairs={{0,16},{4,20},{8,24},{12,28},{16,0},{20,4},{24,8},{28,12},{1,17},{... | collective-permute-start | bytes 2162696 | tf_op jit(solution)/shard_map/ppermute | solution.py:25
  420.5 90.3 %collective-permute-start.21 = (bf16[1408,256]{1,0:T(8,128)(2,1)}, bf16[1408,256]{1,0:T(8,128)(2,1)}, u32[]{:S(2)}, u32[]{:S(2)}) collective-permute-start(bf16[1408,256]{1,0:T(8,128)(2,1)} %param.34), channel_id=1, source_target_pairs={{0,12},{4,16},{8,20},{12,24},{16,28},{20,0},{24,4},{28,8},{1,13},{... | collective-permute-start | bytes 2162696 | tf_op jit(solution)/shard_map/ppermute | solution.py:25
  441.0 8.0 %copy-start.4 = (bf16[768,1408]{1,0:T(8,128)(2,1)S(1)}, bf16[768,1408]{1,0:T(8,128)(2,1)}, u32[]{:S(2)}) copy-start(bf16[768,1408]{1,0:T(8,128)(2,1)} %convolution_convert_fusion.1) | copy-start | bytes 6488068
  451.1 60.9 %collective-permute-start.22 = (bf16[1408,256]{1,0:T(8,128)(2,1)}, bf16[1408,256]{1,0:T(8,128)(2,1)S(1)}, u32[]{:S(2)}, u32[]{:S(2)}) collective-permute-start(bf16[1408,256]{1,0:T(8,128)(2,1)} %param.34), channel_id=1, source_target_pairs={{0,8},{4,12},{8,16},{12,20},{16,24},{20,28},{24,0},{28,4},{1,9},{5... | collective-permute-start | bytes 2162696 | tf_op jit(solution)/shard_map/ppermute | solution.py:25
  452.4 59.8 %collective-permute-start.23 = (bf16[1408,256]{1,0:T(8,128)(2,1)}, bf16[1408,256]{1,0:T(8,128)(2,1)S(1)}, u32[]{:S(2)}, u32[]{:S(2)}) collective-permute-start(bf16[1408,256]{1,0:T(8,128)(2,1)} %param.34), channel_id=1, source_target_pairs={{0,4},{4,8},{8,12},{12,16},{16,20},{20,24},{24,28},{28,0},{1,5},{5... | collective-permute-start | bytes 2162696 | tf_op jit(solution)/shard_map/ppermute | solution.py:25
  455.1 57.2 %collective-permute-start.16 = (bf16[2,2816]{1,0:T(2,128)(2,1)S(1)}, bf16[2,2816]{1,0:T(2,128)(2,1)S(1)}, u32[]{:S(2)}, u32[]{:S(2)}) collective-permute-start(bf16[2,2816]{1,0:T(2,128)(2,1)S(1)} %pad_maximum_fusion.5), channel_id=1, source_target_pairs={{0,4},{4,8},{8,12},{12,16},{16,20},{20,24},{24,28},{1,5},{5,9},{9,... | collective-permute-start | bytes 33800 | tf_op jit(solution)/shard_map/ppermute | solution.py:20
  520.9 38.1 %copy-start.15 = (f32[2048]{0:T(1024)S(1)}, f32[2048]{0:T(1024)}, u32[]{:S(2)}) copy-start(f32[2048]{0:T(1024)} %param.35) | copy-start | bytes 24580
  520.9 20.5 %collective-permute-start.24 = (bf16[192,2048]{1,0:T(8,128)(2,1)S(1)}, bf16[192,2048]{1,0:T(8,128)(2,1)S(1)}, u32[]{:S(2)}, u32[]{:S(2)}) collective-permute-start(bf16[192,2048]{1,0:T(8,128)(2,1)S(1)} %convolution_convert_fusion.4), channel_id=1, source_target_pairs={{0,2},{1,3},{2,0},{3,1},{4,6},{5,7},{6,4},{7,5},{8,10},{9,11},{10,... | collective-permute-start | bytes 2359304 | tf_op jit(solution)/shard_map/ppermute | solution.py:25
  522.0 33.7 %collective-permute-start.25 = (bf16[192,2048]{1,0:T(8,128)(2,1)S(1)}, bf16[192,2048]{1,0:T(8,128)(2,1)S(1)}, u32[]{:S(2)}, u32[]{:S(2)}) collective-permute-start(bf16[192,2048]{1,0:T(8,128)(2,1)S(1)} %convolution_convert_fusion.3), channel_id=1, source_target_pairs={{0,1},{1,2},{2,3},{3,0},{4,5},{5,6},{6,7},{7,4},{8,9},{9,10},{10,1... | collective-permute-start | bytes 2359304 | tf_op jit(solution)/shard_map/ppermute | solution.py:25
  522.0 33.7 %collective-permute-start.26 = (bf16[192,2048]{1,0:T(8,128)(2,1)S(1)}, bf16[192,2048]{1,0:T(8,128)(2,1)S(1)}, u32[]{:S(2)}, u32[]{:S(2)}) collective-permute-start(bf16[192,2048]{1,0:T(8,128)(2,1)S(1)} %convolution_convert_fusion.2), channel_id=1, source_target_pairs={{0,3},{1,0},{2,1},{3,2},{4,7},{5,4},{6,5},{7,6},{8,11},{9,8},{10,9... | collective-permute-start | bytes 2359304 | tf_op jit(solution)/shard_map/ppermute | solution.py:25
Sparse Core Ops, SparseCore 0:
  9.5 119.0 all-gather.2
  130.8 142.3 all-gather.4
